TPU v7x, 256 devices: a whole 4x4x8 slice. The times are simulated.
256 devices in a mesh: sp: 32 (over z, x), tp: 8 (over y, core).
Axes of the slice: x: 4, y: 4, z: 8, core: 2. Of those that a mesh axis runs over, the one named last changes fastest.
Arguments:
- residual: bfloat16 [24576, 2048], P('sp'), may hold values from -6 to 6
- queries: bfloat16 [24576, 1024], P('sp', 'tp'), may hold values from -12 to 12
- keys: bfloat16 [24576, 512], P('sp', 'tp'), may hold values from -6 to 6
- values: bfloat16 [24576, 512], P('sp', 'tp'), may hold values from -36 to 36
- segments: int32 [24576], P('sp'), may hold values from 0 to 15, never falling along the last dimension, each value on 1 to 3072 neighbouring positions
- sink: float32 [16], P('tp'), may hold values from 3 to 7
- out_weight: bfloat16 [1024, 2048], replicated, may hold values from -0.1875 to 0.1875
- norm_gain_one: float32 [2048], replicated, may hold values from 0.1 to 1.9
- group: int32 [24576], P('sp'), may hold values from 0 to 3, as said below
- member: int32 [24576, 2], P('sp'), may hold values from 0 to 7, as said below
- route_weight: float32 [24576, 2], P('sp'), may hold values from 0.25 to 1
- gate_weight: bfloat16 [32, 2048, 1024], P('sp', None, 'tp'), may hold values from -0.125 to 0.125
- up_weight: bfloat16 [32, 2048, 1024], P('sp', None, 'tp'), may hold values from -0.125 to 0.125
- down_weight: bfloat16 [32, 1024, 2048], P('sp', None, 'tp'), may hold values from -0.1875 to 0.1875
- norm_gain_two: float32 [2048], P('tp'), may hold values from 0.1 to 1.9
Outputs:
- output: bfloat16 [24576, 2048], P('sp', 'tp')
Inputs may be any that keep to these rules, and one draw needn't show every extreme that they name: In every aligned block of 96 rows no expert (group * 8 + member) is named by more than 12 rows, and one expert, the same in all blocks of a draw, is named by exactly 12 rows of every block. `member`: the 2 members of a row differ.
All inputs are finite; a program needn't handle non-finite values.
Results may differ from a plain program's by a relative error of at most 0.0059.
Values may be sent and summed in bfloat16 or wider, within the bound.
No kernel may reach another device: no remote copies, remote signals or barrier semaphores. Data moves between devices by JAX's collectives and lax.ppermute only.
A program may use at most 128 MiB of HBM per device.

v0:
```python
import math
import jax
import jax.numpy as jnp
from jax import lax
from jax.sharding import PartitionSpec as P

HEAD_DIM = 64
HALF = 128
PER_GROUP = 8
ALPHA = 2.0**0.25
EPS = 1e-05


def with_halo(block, sides, width):
    for axis, dim in sides:
        count = lax.axis_size(axis)
        forward = [(i, i + 1) for i in range(count - 1)]
        backward = [(target, source) for source, target in forward]
        low = lax.ppermute(
            lax.slice_in_dim(block, block.shape[dim] - width, None, axis=dim), axis, forward
        )
        high = lax.ppermute(lax.slice_in_dim(block, 0, width, axis=dim), axis, backward)
        block = jnp.concatenate([low, block, high], axis=dim)
    return block


def copy_for_each(x, axis):
    copies = jnp.broadcast_to(x, (lax.axis_size(axis), *x.shape))
    return lax.all_to_all(copies, axis, split_axis=0, concat_axis=0, tiled=True)


def joined_along(pieces, dim):
    pieces = jnp.moveaxis(pieces, 0, dim)
    lengths = pieces.shape
    return pieces.reshape(*lengths[:dim], lengths[dim] * lengths[dim + 1], *lengths[dim + 2 :])


def gather_directly(x, axis, dim):
    pieces = copy_for_each(x, axis)
    return joined_along(pieces, dim)


def taken_together(x, axis):
    everything = copy_for_each(x, axis)
    return jnp.sum(everything, axis=0)


def packed_total(arrays, axis):
    ends = [0]
    for a in arrays:
        ends.append(ends[-1] + a.size)
    subtotal = taken_together(jnp.concatenate([a.ravel() for a in arrays]), axis)
    return tuple((subtotal[b:e].reshape(a.shape) for a, b, e in zip(arrays, ends, ends[1:])))


def layer_norm(summed, norm_gain):
    mean_value = jnp.mean(summed, -1, keepdims=True)
    variance = jnp.mean(jnp.square(summed - mean_value), -1, keepdims=True)
    return ((summed - mean_value) * lax.rsqrt(variance + EPS) * norm_gain).astype(jnp.bfloat16)


def shards(
    residual,
    queries,
    keys,
    values,
    segments,
    sink,
    out_weight,
    norm_gain_one,
    group,
    member,
    route_weight,
    gate_weight,
    up_weight,
    down_weight,
    norm_gain_two,
):
    row_count = queries.shape[0]
    sp_size = lax.axis_size("sp")
    tp_size = lax.axis_size("tp")
    kv_local = keys.shape[1] // HEAD_DIM
    heads_local = queries.shape[1] // HEAD_DIM
    group_size = heads_local // kv_local
    seq_total = row_count * sp_size
    seq_start = lax.axis_index("sp") * row_count
    joined = jnp.concatenate([keys, values], axis=1)
    padded, seg_padded = (
        with_halo(joined, (("sp", 0),), HALF),
        with_halo(segments, (("sp", 0),), HALF),
    )
    query_block = math.gcd(row_count, 512)
    key_span = query_block + 2 * HALF
    offsets = jnp.arange(key_span)[None, :] - HALF - jnp.arange(query_block)[:, None]
    in_band = jnp.abs(offsets) <= HALF
    sink_heads = sink.reshape(kv_local, group_size, 1, 1)
    query_heads = queries.reshape(row_count, kv_local, group_size, HEAD_DIM)
    key_cols = kv_local * HEAD_DIM
    pieces = []
    for number in range(row_count // query_block):
        row_low = number * query_block
        query_rows = query_heads[row_low : row_low + query_block]
        kv_rows = padded[row_low : row_low + key_span]
        key_part = kv_rows[:, :key_cols].reshape(key_span, kv_local, HEAD_DIM)
        value_part = kv_rows[:, key_cols:].reshape(key_span, kv_local, HEAD_DIM)
        key_place = seq_start + row_low - HALF + jnp.arange(key_span)
        inside = (key_place >= 0) & (key_place < seq_total)
        same_doc = (
            segments[row_low : row_low + query_block, None]
            == seg_padded[None, row_low : row_low + key_span]
        )
        allowed = in_band & same_doc & inside[None, :]
        scores = jnp.einsum(
            "qkgd,ckd->kgqc", query_rows, key_part, preferred_element_type=jnp.float32
        ) * HEAD_DIM ** (-0.5)
        masked = jnp.where(allowed, scores, -1e30)
        peak = jnp.maximum(jnp.max(masked, -1, keepdims=True), sink_heads)
        raised = jnp.where(allowed, jnp.exp(masked - peak), 0.0)
        denominator = jnp.sum(raised, -1, keepdims=True) + jnp.exp(sink_heads - peak)
        weights = (raised / denominator).astype(jnp.bfloat16)
        attended_part = jnp.einsum(
            "kgqc,ckd->qkgd", weights, value_part, preferred_element_type=jnp.float32
        )
        pieces.append(
            attended_part.reshape(query_block, heads_local * HEAD_DIM).astype(jnp.bfloat16)
        )
    attended = jnp.concatenate(pieces, 0)
    width = out_weight.shape[1]
    weight_rows = out_weight
    mixed = jnp.dot(
        gather_directly(attended, "tp", 1), weight_rows, preferred_element_type=jnp.float32
    )
    pre_one = ALPHA * residual.astype(jnp.float32) + mixed
    normed = layer_norm(pre_one, norm_gain_one)
    experts_local = gate_weight.shape[0]
    expert_count = experts_local * sp_size
    picks_count = member.shape[1]
    block_rows = row_count // tp_size
    capacity = max(2, block_rows // 8)
    expert_ids = (group[:, None] * PER_GROUP + member).reshape(tp_size, block_rows * picks_count)
    onehot_table = (expert_ids[:, :, None] == jnp.arange(expert_count)[None, None, :]).astype(
        jnp.int32
    )
    ranks = jnp.sum((jnp.cumsum(onehot_table, 1) - 1) * onehot_table, 2)
    owner = expert_ids // experts_local
    local_ids = expert_ids % experts_local
    block_ids = jnp.arange(tp_size)[:, None]
    slot_all = ((local_ids * sp_size + owner) * tp_size + block_ids) * capacity + ranks
    copy_rows = (
        jnp.arange(row_count * picks_count).reshape(tp_size, block_rows * picks_count)
        // picks_count
    )
    extended = jnp.concatenate([normed, jnp.zeros((1, width), jnp.bfloat16)], 0)
    tp_place = lax.axis_index("tp")
    slot_own_base = (local_ids * sp_size + owner) * capacity + ranks
    own_slots = lax.dynamic_index_in_dim(slot_own_base, tp_place, 0, keepdims=False)
    own_rows = lax.dynamic_index_in_dim(copy_rows, tp_place, 0, keepdims=False)
    slot_count = experts_local * sp_size * capacity
    source = jnp.full((slot_count,), row_count, jnp.int32).at[own_slots].set(own_rows)
    outgoing = extended[source].reshape(experts_local, sp_size, capacity, width)
    received = lax.all_to_all(outgoing, "sp", split_axis=1, concat_axis=1, tiled=True)
    arrived = lax.all_gather(received, "tp", axis=2, tiled=True)
    expert_rows = arrived.reshape(experts_local, sp_size * tp_size * capacity, width)
    gate_part = jnp.einsum(
        "esd,edf->esf", expert_rows, gate_weight, preferred_element_type=jnp.float32
    )
    up_part = jnp.einsum("esd,edf->esf", expert_rows, up_weight, preferred_element_type=jnp.float32)
    hidden = (jax.nn.silu(gate_part) * up_part).astype(jnp.bfloat16)
    column_width = down_weight.shape[2]
    weight_rows = down_weight
    produced = jnp.einsum(
        "esf,efc->esc",
        lax.all_gather(hidden, "tp", axis=2, tiled=True),
        weight_rows,
        preferred_element_type=jnp.float32,
    ).astype(jnp.bfloat16)
    returned = lax.all_to_all(
        produced.reshape(experts_local, sp_size, tp_size * capacity, column_width),
        "sp",
        split_axis=1,
        concat_axis=1,
        tiled=True,
    )
    result_rows = returned.reshape(-1, column_width)
    picked = result_rows[slot_all.reshape(row_count, picks_count)]
    combined = jnp.sum(route_weight[:, :, None] * picked.astype(jnp.float32), 1)
    column_start = lax.axis_index("tp") * column_width
    normed_part = lax.dynamic_slice_in_dim(normed, column_start, column_width, 1)
    pre_two = ALPHA * normed_part.astype(jnp.float32) + combined
    sums, squares = packed_total((jnp.sum(pre_two, -1), jnp.sum(pre_two * pre_two, -1)), "tp")
    mean_value = (sums / width)[:, None]
    variance = (squares / width)[:, None] - mean_value * mean_value
    return ((pre_two - mean_value) * lax.rsqrt(variance + EPS) * norm_gain_two).astype(jnp.bfloat16)


def solution(mesh):
    in_specs = (
        P("sp", None),
        P("sp", "tp"),
        P("sp", "tp"),
        P("sp", "tp"),
        P("sp"),
        P("tp"),
        P(),
        P(),
        P("sp"),
        P("sp", None),
        P("sp", None),
        P("sp", None, "tp"),
        P("sp", None, "tp"),
        P("sp", None, "tp"),
        P("tp"),
    )
    out_specs = P("sp", "tp")
    return jax.shard_map(shards, mesh=mesh, in_specs=in_specs, out_specs=out_specs, check_vma=False)
```

profile of v0, /device:TPU:1, one launch (start us, length us, event | category | flops | bytes accessed | tf_op | source)
XLA Modules:
  0.0 366.8 jit_solution(6680165087132534622)
XLA Ops:
  6.5 0.8 fusion.64
  7.4 3.9 %collective-permute-start.1 = (s32[128]{0:T(128)S(1)}, s32[128]{0:T(128)S(1)}, u32[]{:S(2)}, u32[]{:S(2)}) collective-permute-start(s32[128]{0:T(128)S(1)} %get-tuple-element.16), channel_id=1, source_target_pairs={{0,8},{8,16},{16,24},{24,32},{32,40},{40,48},{48,56},{56,64},{64,7... | collective-permute-start | bytes 1544 | tf_op jit(solution)/shard_map/ppermute | solution.py:19
  11.3 1.3 collective-permute-start.3
  12.6 0.9 constant_dynamic-update-slice_fusion.1
  13.5 0.9 constant_dynamic-update-slice_fusion
  14.4 4.0 %collective-permute-start = (bf16[128,128]{0,1:T(8,128)(2,1)S(1)}, bf16[128,128]{0,1:T(8,128)(2,1)S(1)}, u32[]{:S(2)}, u32[]{:S(2)}) collective-permute-start(bf16[128,128]{0,1:T(8,128)(2,1)S(1)} %get-tuple-element.7), channel_id=1, source_target_pairs={{0,8},{8,16},{16,24},{24,32},{32,40},{40,48},{48,56},{56,64},{64,7... | collective-permute-start | bytes 98312 | tf_op jit(solution)/shard_map/ppermute | solution.py:19
  18.4 1.3 collective-permute-start.2
  19.7 0.8 fusion.65
  20.5 0.7 broadcast_multiply_fusion
  21.2 0.9 fusion.63
  22.1 0.9 copy.90
  23.0 0.2 broadcast_add_fusion
  23.2 0.2 reshape.414
  23.5 0.7 slice.98
  24.2 0.1 copy.83
  24.3 0.1 copy.87
  24.4 0.1 copy.85
  24.6 0.7 and_and_fusion.2
  25.4 0.3 fusion.67
  25.7 0.3 fusion.66
  26.1 0.2 fusion.7
  26.4 0.3 fusion.68
  26.8 0.2 fusion.8
  27.0 0.2 fusion.9
  27.2 0.1 exponential_add_fusion.1
  27.3 0.4 convolution_convert_fusion.1
  27.7 0.4 convolution_convert_fusion.3
  28.1 0.4 convolution_convert_fusion.2
  28.5 1.3 broadcast_in_dim.73
  29.7 6.0 %all-to-all-start = ((bf16[8,768,128]{1,2,0:T(8,128)(2,1)}), bf16[8,768,128]{1,2,0:T(8,128)(2,1)S(1)}, u32[]{:S(2)}, u32[]{:S(2)}) async-start(bf16[8,768,128]{1,2,0:T(8,128)(2,1)} %broadcast_in_dim.73), calls=%async_computation | async-start | bytes 3145728 | tf_op jit(solution)/shard_map/all_to_all | solution.py:29
  35.7 4.6 %reduce-window.6 = s32[8,32,2,128]{3,1,2,0:T(8,128)S(1)} reduce-window(s32[8,32,2,128]{3,1,2,0:T(8,128)S(1)} %copy_bitcast_fusion, s32[]{:T(128)} %constant.104.clone.1), window={size=1x1x1x128 pad=0_0x0_0x0_0x127_0}, to_apply=%region_8.9 | reduce-window | flops 8323072 | bytes 524292 | tf_op jit(solution)/shard_map/reduce-window
  40.4 0.1 slice.120
  40.5 0.2 copy.92
  40.7 0.1 bitcast_bitcast_fusion
  41.0 1.4 scatter_custom_fusion
  42.4 13.9 %all-to-all-done = bf16[8,768,128]{1,2,0:T(8,128)(2,1)S(1)} async-done(((bf16[8,768,128]{1,2,0:T(8,128)(2,1)}), bf16[8,768,128]{1,2,0:T(8,128)(2,1)S(1)}, u32[]{:S(2)}, u32[]{:S(2)}) %all-to-all-start) | async-done | bytes 1572896 | tf_op jit(solution)/shard_map/all_to_all | solution.py:29
  56.3 7.3 %fusion.69 = (f32[768]{0:T(1024)S(1)}, f32[768,2048]{1,0:T(8,128)S(1)}) fusion(bf16[768,1024]{0,1:T(8,128)(2,1)S(1)} %bitcast.123, bf16[1024,2048]{1,0:T(8,128)(2,1)} %param.21, bf16[768,2048]{1,0:T(8,128)(2,1)} %param.15), kind=kOutput, calls=%fused_computation.143 | convolution fusion | flops 3227516160 | bytes 15207424 | tf_op jit(solution)/shard_map/dot_general | solution.py:130
  63.7 0.8 multiply_reduce_fusion
  64.5 0.9 multiply_convert_fusion
  65.4 1.7 copy-done.1
  67.0 2.0 concatenate.32
  69.1 7.4 %gather_fusion = bf16[384,2048]{1,0:T(8,128)(2,1)} fusion(bf16[769,2048]{1,0:T(8,128)(2,1)} %concatenate.32, s32[1024]{0:T(1024)S(1)} %pad_clamp_fusion.1), kind=kCustom, calls=%fused_computation | custom fusion | bytes 3147264 | tf_op jit(solution)/shard_map/gather | solution.py:160
  76.4 2.4 reshape.420
  78.8 64.7 %all_to_all.21 = bf16[1,32,12,2048]{3,2,0,1:T(8,128)(2,1)S(1)} all-to-all(bf16[1,32,12,2048]{3,2,0,1:T(8,128)(2,1)S(1)} %bitcast.122), channel_id=1, replica_groups=mesh['sp'=32,'tp'=8] {'sp'}, dimensions={1} | all-to-all | bytes 3145728 | tf_op jit(solution)/shard_map/all_to_all | solution.py:161
  143.5 2.0 copy.96
  145.5 0.3 all-gather.6.cloned.1.call-start
  145.8 67.6 %all-gather.4.cloned.1.call-done = bf16[1,32,96,2048]{3,1,0,2:T(8,128)(2,1)} async-done(((bf16[1,32,12,2048]{3,1,0,2:T(8,128)(2,1)}), bf16[1,32,96,2048]{3,1,0,2:T(8,128)(2,1)}) %all-gather.4.cloned.1.call-update) | async-done | bytes 12582928 | tf_op jit(solution)/shard_map/all_gather | solution.py:162
  213.4 11.7 %copy.97 = bf16[1,32,96,2048]{3,2,1,0:T(8,128)(2,1)S(1)} copy(bf16[1,32,96,2048]{3,1,0,2:T(8,128)(2,1)} %all-gather.4.cloned.1.call-done) | data formatting | bytes 25165824 | tf_op jit(solution)/shard_map/all_gather | solution.py:162
  225.2 3.5 fusion.12
  228.7 4.5 %fusion = bf16[3072,128]{1,0:T(8,128)(2,1)} fusion(bf16[3072,2048]{1,0:T(8,128)(2,1)S(1)} %bitcast.121, f32[3072,128]{1,0:T(8,128)S(1)} %fusion.12, bf16[1,2048,128]{2,1,0:T(8,128)(2,1)S(1)} %copy-done.10), kind=kOutput, calls=%fused_computation.8 | convolution fusion | flops 1612972032 | bytes 15466496 | tf_op jit(solution)/shard_map/esd,edf->esf/dot_general | solution.py:167
  233.2 47.5 %all-gather.6.cloned.1.call-done = bf16[3072,1024]{1,0:T(8,128)(2,1)} async-done(((bf16[3072,128]{1,0:T(8,128)(2,1)}), bf16[3072,1024]{1,0:T(8,128)(2,1)}) %all-gather.6.cloned.1.call-update) | async-done | bytes 6291472 | tf_op jit(solution)/shard_map/all_gather | solution.py:173
  280.8 5.7 %convolution_convert_fusion = bf16[3072,256]{1,0:T(8,128)(2,1)} fusion(bf16[3072,1024]{1,0:T(8,128)(2,1)} %all-gather.6.cloned.1.call-done, bf16[1,1024,256]{2,1,0:T(8,128)(2,1)S(1)} %copy-done), kind=kOutput, calls=%fused_computation.6 | convolution fusion | flops 1611399168 | bytes 8388608 | tf_op jit(solution)/shard_map/esf,efc->esc/dot_general | solution.py:171
  286.5 9.9 %all-to-all-start.2 = ((bf16[1,32,96,256]{3,2,0,1:T(8,128)(2,1)}), bf16[1,32,96,256]{3,2,0,1:T(8,128)(2,1)S(1)}, u32[]{:S(2)}, u32[]{:S(2)}) async-start(bf16[1,32,96,256]{3,2,0,1:T(8,128)(2,1)} %bitcast.124), calls=%async_computation.2 | async-start | bytes 3145728 | tf_op jit(solution)/shard_map/all_to_all | solution.py:177
  296.4 0.3 reduce_sum.98
  296.9 0.3 compare_select_fusion
  297.1 0.2 reshape.439
  297.4 0.2 copy.89
  297.6 36.4 %all-to-all-done.2 = bf16[1,32,96,256]{3,2,0,1:T(8,128)(2,1)S(1)} async-done(((bf16[1,32,96,256]{3,2,0,1:T(8,128)(2,1)}), bf16[1,32,96,256]{3,2,0,1:T(8,128)(2,1)S(1)}, u32[]{:S(2)}, u32[]{:S(2)}) %all-to-all-start.2) | async-done | bytes 1572896 | tf_op jit(solution)/shard_map/all_to_all | solution.py:177
  334.0 5.3 %gather_fusion.1 = bf16[1536,256]{1,0:T(8,128)(2,1)} fusion(bf16[3072,256]{1,0:T(8,128)(2,1)S(1)} %bitcast.119, s32[2048]{0:T(1024)S(1)} %pad_clamp_fusion), kind=kCustom, calls=%fused_computation.1 | custom fusion | bytes 1579008 | tf_op jit(solution)/shard_map/gather | solution.py:185
  339.3 2.2 reshape.458
  341.5 4.2 %multiply_reduce_fusion.1 = f32[768,256]{1,0:T(8,128)S(1)} fusion(f32[768,2,256]{2,1,0:T(2,128)S(1)} %reshape.458, f32[768,2]{1,0:T(8,128)S(1)} %copy.89), kind=kLoop, calls=%fused_computation.9 | loop fusion | flops 589824 | bytes 2365440 | tf_op jit(solution)/shard_map/reduce_sum | solution.py:186
  345.7 1.3 fusion.19
  347.1 10.8 %all_to_all.22 = f32[8,1,1536]{2,1,0:T(1,128)S(1)} all-to-all(f32[8,1,1536]{2,1,0:T(1,128)S(1)} %broadcast_in_dim.77), channel_id=1, replica_groups=mesh['sp'=32,'tp'=8] {'tp'}, dimensions={0} | all-to-all | bytes 98304 | tf_op jit(solution)/shard_map/all_to_all | solution.py:29
  357.9 2.0 multiply_convert_fusion.1
  (59 shorter events, 0.7 us)
Async XLA Ops:
  6.5 274.2 %copy-start = (bf16[1,1024,256]{2,1,0:T(8,128)(2,1)S(1)}, bf16[1,1024,256]{2,1,0:T(8,128)(2,1)}, u32[]{:S(2)}) copy-start(bf16[1,1024,256]{2,1,0:T(8,128)(2,1)} %param.28) | copy-start | bytes 1572868
  6.5 18.0 %copy-start.4 = (s32[768]{0:T(1024)S(1)}, s32[768]{0:T(1024)}, u32[]{:S(2)}) copy-start(s32[768]{0:T(1024)} %param.19) | copy-start | bytes 9220
  6.5 18.8 %copy-start.2 = (bf16[768,64]{0,1:T(8,128)(2,1)S(1)}, bf16[768,64]{0,1:T(8,128)(2,1)}, u32[]{:S(2)}) copy-start(bf16[768,64]{0,1:T(8,128)(2,1)} %param.17) | copy-start | bytes 294916
  7.4 17.2 %collective-permute-start.1 = (s32[128]{0:T(128)S(1)}, s32[128]{0:T(128)S(1)}, u32[]{:S(2)}, u32[]{:S(2)}) collective-permute-start(s32[128]{0:T(128)S(1)} %get-tuple-element.16), channel_id=1, source_target_pairs={{0,8},{8,16},{16,24},{24,32},{32,40},{40,48},{48,56},{56,64},{64,7... | collective-permute-start | bytes 1544 | tf_op jit(solution)/shard_map/ppermute | solution.py:19
  11.3 13.3 %collective-permute-start.3 = (s32[128]{0:T(128)S(1)}, s32[128]{0:T(128)S(1)}, u32[]{:S(2)}, u32[]{:S(2)}) collective-permute-start(s32[128]{0:T(128)S(1)} %get-tuple-element.17), channel_id=1, source_target_pairs={{8,0},{16,8},{24,16},{32,24},{40,32},{48,40},{56,48},{64,56},{72,6... | collective-permute-start | bytes 1544 | tf_op jit(solution)/shard_map/ppermute | solution.py:22
  14.4 11.7 %copy-start.7 = (f32[2]{0:T(128)S(1)}, f32[2]{0:T(128)}, u32[]{:S(2)}) copy-start(f32[2]{0:T(128)} %param.20) | copy-start | bytes 28
  14.4 11.3 %collective-permute-start = (bf16[128,128]{0,1:T(8,128)(2,1)S(1)}, bf16[128,128]{0,1:T(8,128)(2,1)S(1)}, u32[]{:S(2)}, u32[]{:S(2)}) collective-permute-start(bf16[128,128]{0,1:T(8,128)(2,1)S(1)} %get-tuple-element.7), channel_id=1, source_target_pairs={{0,8},{8,16},{16,24},{24,32},{32,40},{40,48},{48,56},{56,64},{64,7... | collective-permute-start | bytes 98312 | tf_op jit(solution)/shard_map/ppermute | solution.py:19
  18.4 7.9 %collective-permute-start.2 = (bf16[128,128]{0,1:T(8,128)(2,1)S(1)}, bf16[128,128]{0,1:T(8,128)(2,1)S(1)}, u32[]{:S(2)}, u32[]{:S(2)}) collective-permute-start(bf16[128,128]{0,1:T(8,128)(2,1)S(1)} %get-tuple-element.8), channel_id=1, source_target_pairs={{8,0},{16,8},{24,16},{32,24},{40,32},{48,40},{56,48},{64,56},{72,6... | collective-permute-start | bytes 98312 | tf_op jit(solution)/shard_map/ppermute | solution.py:22
  25.7 1.6 copy-start.3
  29.7 26.6 %all-to-all-start = ((bf16[8,768,128]{1,2,0:T(8,128)(2,1)}), bf16[8,768,128]{1,2,0:T(8,128)(2,1)S(1)}, u32[]{:S(2)}, u32[]{:S(2)}) async-start(bf16[8,768,128]{1,2,0:T(8,128)(2,1)} %broadcast_in_dim.73), calls=%async_computation | async-start | bytes 3145728 | tf_op jit(solution)/shard_map/all_to_all | solution.py:29
  35.7 177.7 %all-gather.4.cloned.1.call-start = ((), (), s32[]{:S(2)}) async-start(), calls=%async_computation.4 | async-start | bytes 14155776 | tf_op jit(solution)/shard_map/all_gather | solution.py:162
  63.7 0.8 copy-start.5
  65.3 1.7 copy-start.1
  145.5 79.6 %copy-start.9 = (bf16[1,2048,128]{2,1,0:T(8,128)(2,1)S(1)}, bf16[1,2048,128]{2,1,0:T(8,128)(2,1)}, u32[]{:S(2)}) copy-start(bf16[1,2048,128]{2,1,0:T(8,128)(2,1)} %param.26) | copy-start | bytes 1572868
  145.5 135.3 %all-gather.6.cloned.1.call-start = ((), (), s32[]{:S(2)}) async-start(), calls=%async_computation.5 | async-start | bytes 7077888 | tf_op jit(solution)/shard_map/all_gather | solution.py:173
  225.1 3.6 copy-start.10
  286.5 10.9 %copy-start.6 = (f32[768,2]{0,1:T(2,128)S(1)}, f32[768,2]{0,1:T(2,128)}, u32[]{:S(2)}) copy-start(f32[768,2]{0,1:T(2,128)} %param.25) | copy-start | bytes 18436
  286.5 47.5 %all-to-all-start.2 = ((bf16[1,32,96,256]{3,2,0,1:T(8,128)(2,1)}), bf16[1,32,96,256]{3,2,0,1:T(8,128)(2,1)S(1)}, u32[]{:S(2)}, u32[]{:S(2)}) async-start(bf16[1,32,96,256]{3,2,0,1:T(8,128)(2,1)} %bitcast.124), calls=%async_computation.2 | async-start | bytes 3145728 | tf_op jit(solution)/shard_map/all_to_all | solution.py:177
  339.3 18.6 %copy-start.8 = (f32[256]{0:T(256)S(1)}, f32[256]{0:T(256)}, u32[]{:S(2)}) copy-start(f32[256]{0:T(256)} %param.29) | copy-start | bytes 3076
Sparse Core Ops, SparseCore 0:
  145.6 67.7 all-gather.3
  233.3 47.3 all-gather.5
where the time goes:
time: 368 us; the launch traced here: 367 us
  waiting for transfers between devices  166 us (45%)
  blocking collectives  75.4 us (20%)
  local copies, waits for them, and re-layouts  44.9 us (12%)
  starting transfers between devices  26.7 us (7%)
  matrix products  23.2 us (6%)
  other arithmetic  17 us (5%)
  between operations  14 us (4%)
    all_gather x1, waiting for transfers between devices, shards(): arrived = lax.all_gather(received, 'tp', axis=2, tiled=True)  67.6 us
    all_to_all x1, blocking collectives, shards(): lax.all_to_all(outgoing, 'sp', split_axis=1, concat_axis=1, tiled=True)  64.7 us
    all_gather x1, waiting for transfers between devices, shards(): lax.all_gather(hidden, 'tp', axis=2, tiled=True)  47.5 us
    all_to_all x1, waiting for transfers between devices, shards(): lax.all_to_all(produced.reshape(experts_local, sp_size, tp_size * capacit...  36.4 us
    all_to_all x1, waiting for transfers between devices, copy_for_each(): return lax.all_to_all(copies, axis, split_axis=0, concat_axis=0, tiled=True)  13.9 us
    all_gather x1, local copies, waits for them, and re-layouts, shards(): arrived = lax.all_gather(received, 'tp', axis=2, tiled=True)  11.7 us
    all_to_all x1, blocking collectives, copy_for_each(): return lax.all_to_all(copies, axis, split_axis=0, concat_axis=0, tiled=True)  10.8 us
    all_to_all x1, starting transfers between devices, shards(): lax.all_to_all(produced.reshape(experts_local, sp_size, tp_size * capacit...  9.93 us
  transfers between devices with their start and end apart: 8, of which 4 were waited for; matrix products, arithmetic and copies ran while one was open for 4% of the time, Pallas kernels for 0%

commit v1 on v0

--- a/solution.py
+++ b/solution.py
@@ -174,12 +174,17 @@
         weight_rows,
         preferred_element_type=jnp.float32,
     ).astype(jnp.bfloat16)
-    returned = lax.all_to_all(
-        produced.reshape(experts_local, sp_size, tp_size * capacity, column_width),
-        "sp",
-        split_axis=1,
-        concat_axis=1,
-        tiled=True,
+    _point_goods = lambda u, shard_axis, array_axis, join_dim: jnp.concatenate(
+        jax.lax.all_to_all(
+            jnp.stack(jnp.split(u, jax.lax.psum(1, axis_name=shard_axis), array_axis)),
+            concat_axis=0,
+            split_axis=0,
+            axis_name=shard_axis,
+        ),
+        join_dim,
+    )
+    returned = _point_goods(
+        produced.reshape(experts_local, sp_size, tp_size * capacity, column_width), "sp", 1, 1
     )
     result_rows = returned.reshape(-1, column_width)
     picked = result_rows[slot_all.reshape(row_count, picks_count)]

time: 368 us -> 386 us (1.049)
  local copies, waits for them, and re-layouts: 44.9 us -> 64.3 us
    unnamed x25 -> x56, local copies, waits for them, and re-layouts: 3.66 us -> 23.1 us
where the time goes in v1:
time: 386 us; the launch traced here: 385 us
  waiting for transfers between devices  166 us (43%)
  blocking collectives  75.4 us (20%)
  local copies, waits for them, and re-layouts  64.3 us (17%)
  starting transfers between devices  26.5 us (7%)
  matrix products  22.1 us (6%)
  other arithmetic  17 us (4%)
  between operations  14 us (4%)
    all_gather x1, waiting for transfers between devices, shards(): arrived = lax.all_gather(received, 'tp', axis=2, tiled=True)  67.6 us
    all_to_all x1, blocking collectives, shards(): lax.all_to_all(outgoing, 'sp', split_axis=1, concat_axis=1, tiled=True)  64.7 us
    all_gather x1, waiting for transfers between devices, shards(): lax.all_gather(hidden, 'tp', axis=2, tiled=True)  47.5 us
    all_to_all x1, waiting for transfers between devices, shards(): jax.lax.all_to_all(jnp.stack(jnp.split(u, jax.lax.psum(1, axis_name=shard...  36.4 us
    unnamed x56, local copies, waits for them, and re-layouts  23.1 us
    all_to_all x1, waiting for transfers between devices, copy_for_each(): return lax.all_to_all(copies, axis, split_axis=0, concat_axis=0, tiled=True)  13.9 us
    all_gather x1, local copies, waits for them, and re-layouts, shards(): arrived = lax.all_gather(received, 'tp', axis=2, tiled=True)  11.7 us
    all_to_all x1, blocking collectives, copy_for_each(): return lax.all_to_all(copies, axis, split_axis=0, concat_axis=0, tiled=True)  10.8 us
  transfers between devices with their start and end apart: 8, of which 4 were waited for; matrix products, arithmetic and copies ran while one was open for 4% of the time, Pallas kernels for 0%

profile of v1, /device:TPU:1, one launch (start us, length us, event | category | flops | bytes accessed | tf_op | source)
XLA Modules:
  0.0 384.9 jit_solution(12500748093466137066)
XLA Ops:
  6.5 0.8 fusion.64
  7.3 3.9 %collective-permute-start.1 = (s32[128]{0:T(128)S(1)}, s32[128]{0:T(128)S(1)}, u32[]{:S(2)}, u32[]{:S(2)}) collective-permute-start(s32[128]{0:T(128)S(1)} %get-tuple-element.16), channel_id=1, source_target_pairs={{0,8},{8,16},{16,24},{24,32},{32,40},{40,48},{48,56},{56,64},{64,7... | collective-permute-start | bytes 1544 | tf_op jit(solution)/shard_map/ppermute | solution.py:19
  11.3 1.3 collective-permute-start.3
  12.6 0.9 constant_dynamic-update-slice_fusion.1
  13.5 0.9 constant_dynamic-update-slice_fusion
  14.4 4.0 %collective-permute-start = (bf16[128,128]{0,1:T(8,128)(2,1)S(1)}, bf16[128,128]{0,1:T(8,128)(2,1)S(1)}, u32[]{:S(2)}, u32[]{:S(2)}) collective-permute-start(bf16[128,128]{0,1:T(8,128)(2,1)S(1)} %get-tuple-element.7), channel_id=1, source_target_pairs={{0,8},{8,16},{16,24},{24,32},{32,40},{40,48},{48,56},{56,64},{64,7... | collective-permute-start | bytes 98312 | tf_op jit(solution)/shard_map/ppermute | solution.py:19
  18.4 1.3 collective-permute-start.2
  19.7 0.8 fusion.65
  20.5 0.7 broadcast_multiply_fusion
  21.2 0.9 fusion.63
  22.1 0.9 copy.87
  24.0 0.7 and_and_fusion.2
  28.1 1.3 broadcast_in_dim.73
  29.3 6.0 %all-to-all-start = ((bf16[8,768,128]{1,2,0:T(8,128)(2,1)}), bf16[8,768,128]{1,2,0:T(8,128)(2,1)S(1)}, u32[]{:S(2)}, u32[]{:S(2)}) async-start(bf16[8,768,128]{1,2,0:T(8,128)(2,1)} %broadcast_in_dim.73), calls=%async_computation | async-start | bytes 3145728 | tf_op jit(solution)/shard_map/all_to_all | solution.py:29
  35.3 4.6 %reduce-window.6 = s32[8,32,2,128]{3,1,2,0:T(8,128)S(1)} reduce-window(s32[8,32,2,128]{3,1,2,0:T(8,128)S(1)} %copy_bitcast_fusion, s32[]{:T(128)} %constant.104.clone.1), window={size=1x1x1x128 pad=0_0x0_0x0_0x127_0}, to_apply=%region_8.9 | reduce-window | flops 8323072 | bytes 524292 | tf_op jit(solution)/shard_map/reduce-window
  40.6 1.4 scatter_custom_fusion
  42.0 13.9 %all-to-all-done = bf16[8,768,128]{1,2,0:T(8,128)(2,1)S(1)} async-done(((bf16[8,768,128]{1,2,0:T(8,128)(2,1)}), bf16[8,768,128]{1,2,0:T(8,128)(2,1)S(1)}, u32[]{:S(2)}, u32[]{:S(2)}) %all-to-all-start) | async-done | bytes 1572896 | tf_op jit(solution)/shard_map/all_to_all | solution.py:29
  55.9 7.3 %fusion.69 = (f32[768]{0:T(1024)S(1)}, f32[768,2048]{1,0:T(8,128)S(1)}) fusion(bf16[768,1024]{0,1:T(8,128)(2,1)S(1)} %bitcast.249, bf16[1024,2048]{1,0:T(8,128)(2,1)} %param.21, bf16[768,2048]{1,0:T(8,128)(2,1)} %param.15), kind=kOutput, calls=%fused_computation.207 | convolution fusion | flops 3227516160 | bytes 15207424 | tf_op jit(solution)/shard_map/dot_general | solution.py:130
  63.3 0.8 multiply_reduce_fusion
  64.0 0.9 multiply_convert_fusion
  64.9 1.7 copy-done.1
  66.6 2.0 concatenate.32
  68.6 7.4 %gather_fusion = bf16[384,2048]{1,0:T(8,128)(2,1)} fusion(bf16[769,2048]{1,0:T(8,128)(2,1)} %concatenate.32, s32[1024]{0:T(1024)S(1)} %pad_clamp_fusion.1), kind=kCustom, calls=%fused_computation | custom fusion | bytes 3147264 | tf_op jit(solution)/shard_map/gather | solution.py:160
  76.0 2.4 reshape.417
  78.4 64.7 %all_to_all.21 = bf16[1,32,12,2048]{3,2,0,1:T(8,128)(2,1)S(1)} all-to-all(bf16[1,32,12,2048]{3,2,0,1:T(8,128)(2,1)S(1)} %bitcast.248), channel_id=1, replica_groups=mesh['sp'=32,'tp'=8] {'sp'}, dimensions={1} | all-to-all | bytes 3145728 | tf_op jit(solution)/shard_map/all_to_all | solution.py:161
  143.0 2.0 copy.93
  145.4 67.6 %all-gather.4.cloned.1.call-done = bf16[1,32,96,2048]{3,1,0,2:T(8,128)(2,1)} async-done(((bf16[1,32,12,2048]{3,1,0,2:T(8,128)(2,1)}), bf16[1,32,96,2048]{3,1,0,2:T(8,128)(2,1)}) %all-gather.4.cloned.1.call-update) | async-done | bytes 12582928 | tf_op jit(solution)/shard_map/all_gather | solution.py:162
  213.0 11.7 %copy.94 = bf16[1,32,96,2048]{3,2,1,0:T(8,128)(2,1)S(1)} copy(bf16[1,32,96,2048]{3,1,0,2:T(8,128)(2,1)} %all-gather.4.cloned.1.call-done) | data formatting | bytes 25165824 | tf_op jit(solution)/shard_map/all_gather | solution.py:162
  224.7 3.5 fusion.12
  228.3 4.5 %fusion = bf16[3072,128]{1,0:T(8,128)(2,1)} fusion(bf16[3072,2048]{1,0:T(8,128)(2,1)S(1)} %bitcast.247, f32[3072,128]{1,0:T(8,128)S(1)} %fusion.12, bf16[1,2048,128]{2,1,0:T(8,128)(2,1)S(1)} %copy-done.10), kind=kOutput, calls=%fused_computation.8 | convolution fusion | flops 1612972032 | bytes 15466496 | tf_op jit(solution)/shard_map/esd,edf->esf/dot_general | solution.py:167
  232.8 47.5 %all-gather.6.cloned.1.call-done = bf16[3072,1024]{1,0:T(8,128)(2,1)} async-done(((bf16[3072,128]{1,0:T(8,128)(2,1)}), bf16[3072,1024]{1,0:T(8,128)(2,1)}) %all-gather.6.cloned.1.call-update) | async-done | bytes 6291472 | tf_op jit(solution)/shard_map/all_gather | solution.py:173
  280.3 4.6 %convolution_convert_fusion = bf16[3072,256]{1,0:T(8,128)(2,1)S(1)} fusion(bf16[3072,1024]{1,0:T(8,128)(2,1)} %all-gather.6.cloned.1.call-done, bf16[1,1024,256]{2,1,0:T(8,128)(2,1)S(1)} %copy-done), kind=kOutput, calls=%fused_computation.6 | convolution fusion | flops 1611399168 | bytes 8388608 | tf_op jit(solution)/shard_map/esf,efc->esc/dot_general | solution.py:171
  284.9 0.6 constant_dynamic-update-slice_fusion.33
  286.2 0.6 constant_dynamic-update-slice_fusion.31
  286.8 0.6 constant_dynamic-update-slice_fusion.30
  287.4 0.6 constant_dynamic-update-slice_fusion.29
  288.6 0.6 constant_dynamic-update-slice_fusion.27
  289.9 0.6 constant_dynamic-update-slice_fusion.25
  290.5 0.6 constant_dynamic-update-slice_fusion.24
  291.7 0.6 constant_dynamic-update-slice_fusion.22
  292.4 0.6 constant_dynamic-update-slice_fusion.21
  293.0 0.6 constant_dynamic-update-slice_fusion.20
  293.6 0.6 constant_dynamic-update-slice_fusion.19
  294.2 0.6 constant_dynamic-update-slice_fusion.18
  294.8 0.6 constant_dynamic-update-slice_fusion.17
  295.4 0.6 constant_dynamic-update-slice_fusion.16
  296.1 0.6 constant_dynamic-update-slice_fusion.15
  296.7 0.6 constant_dynamic-update-slice_fusion.14
  297.3 0.6 constant_dynamic-update-slice_fusion.13
  298.5 0.6 constant_dynamic-update-slice_fusion.11
  299.8 0.6 constant_dynamic-update-slice_fusion.9
  300.4 0.6 constant_dynamic-update-slice_fusion.8
  301.0 0.6 constant_dynamic-update-slice_fusion.7
  302.3 0.6 constant_dynamic-update-slice_fusion.5
  303.5 0.6 constant_dynamic-update-slice_fusion.3
  304.1 0.6 constant_dynamic-update-slice_fusion.2
  304.7 9.8 %all-to-all-start.2 = ((bf16[32,1,1,96,256]{4,3,2,1,0:T(8,128)(2,1)}), bf16[32,1,1,96,256]{4,3,2,1,0:T(8,128)(2,1)S(1)}, u32[]{:S(2)}, u32[]{:S(2)}) async-start(bf16[32,1,1,96,256]{4,3,2,1,0:T(8,128)(2,1)} %constant_dynamic-update-slice_fusion.2), calls=%async_computation.2 | async-start | bytes 3145728 | tf_op jit(solution)/shard_map/all_to_all | solution.py:178
  315.7 36.4 %all-to-all-done.2 = bf16[32,1,1,96,256]{4,3,2,1,0:T(8,128)(2,1)S(1)} async-done(((bf16[32,1,1,96,256]{4,3,2,1,0:T(8,128)(2,1)}), bf16[32,1,1,96,256]{4,3,2,1,0:T(8,128)(2,1)S(1)}, u32[]{:S(2)}, u32[]{:S(2)}) %all-to-all-start.2) | async-done | bytes 1572896 | tf_op jit(solution)/shard_map/all_to_all | solution.py:178
  352.1 5.3 %gather_fusion.1 = bf16[1536,256]{1,0:T(8,128)(2,1)} fusion(bf16[3072,256]{1,0:T(8,128)(2,1)S(1)} %bitcast.245, s32[2048]{0:T(1024)S(1)} %pad_clamp_fusion), kind=kCustom, calls=%fused_computation.1 | custom fusion | bytes 1579008 | tf_op jit(solution)/shard_map/gather | solution.py:190
  357.4 2.1 reshape.454
  359.6 4.2 %multiply_reduce_fusion.1 = f32[768,256]{1,0:T(8,128)S(1)} fusion(f32[768,2,256]{2,1,0:T(2,128)S(1)} %reshape.454, f32[768,2]{1,0:T(8,128)S(1)} %copy.86), kind=kLoop, calls=%fused_computation.9 | loop fusion | flops 589824 | bytes 2365440 | tf_op jit(solution)/shard_map/reduce_sum | solution.py:191
  363.8 1.3 fusion.19
  365.2 10.8 %all_to_all.22 = f32[8,1,1536]{2,1,0:T(1,128)S(1)} all-to-all(f32[8,1,1536]{2,1,0:T(1,128)S(1)} %broadcast_in_dim.77), channel_id=1, replica_groups=mesh['sp'=32,'tp'=8] {'tp'}, dimensions={0} | all-to-all | bytes 98304 | tf_op jit(solution)/shard_map/all_to_all | solution.py:29
  376.0 2.0 multiply_convert_fusion.1
  (91 shorter events, 11.2 us)
Async XLA Ops:
  6.5 273.8 %copy-start = (bf16[1,1024,256]{2,1,0:T(8,128)(2,1)S(1)}, bf16[1,1024,256]{2,1,0:T(8,128)(2,1)}, u32[]{:S(2)}) copy-start(bf16[1,1024,256]{2,1,0:T(8,128)(2,1)} %param.28) | copy-start | bytes 1572868
  6.5 17.0 %copy-start.4 = (s32[768]{0:T(1024)S(1)}, s32[768]{0:T(1024)}, u32[]{:S(2)}) copy-start(s32[768]{0:T(1024)} %param.19) | copy-start | bytes 9220
  7.3 16.5 %collective-permute-start.1 = (s32[128]{0:T(128)S(1)}, s32[128]{0:T(128)S(1)}, u32[]{:S(2)}, u32[]{:S(2)}) collective-permute-start(s32[128]{0:T(128)S(1)} %get-tuple-element.16), channel_id=1, source_target_pairs={{0,8},{8,16},{16,24},{24,32},{32,40},{40,48},{48,56},{56,64},{64,7... | collective-permute-start | bytes 1544 | tf_op jit(solution)/shard_map/ppermute | solution.py:19
  11.3 12.6 %collective-permute-start.3 = (s32[128]{0:T(128)S(1)}, s32[128]{0:T(128)S(1)}, u32[]{:S(2)}, u32[]{:S(2)}) collective-permute-start(s32[128]{0:T(128)S(1)} %get-tuple-element.17), channel_id=1, source_target_pairs={{8,0},{16,8},{24,16},{32,24},{40,32},{48,40},{56,48},{64,56},{72,6... | collective-permute-start | bytes 1544 | tf_op jit(solution)/shard_map/ppermute | solution.py:22
  14.4 10.6 %collective-permute-start = (bf16[128,128]{0,1:T(8,128)(2,1)S(1)}, bf16[128,128]{0,1:T(8,128)(2,1)S(1)}, u32[]{:S(2)}, u32[]{:S(2)}) collective-permute-start(bf16[128,128]{0,1:T(8,128)(2,1)S(1)} %get-tuple-element.7), channel_id=1, source_target_pairs={{0,8},{8,16},{16,24},{24,32},{32,40},{40,48},{48,56},{56,64},{64,7... | collective-permute-start | bytes 98312 | tf_op jit(solution)/shard_map/ppermute | solution.py:19
  18.4 7.3 %collective-permute-start.2 = (bf16[128,128]{0,1:T(8,128)(2,1)S(1)}, bf16[128,128]{0,1:T(8,128)(2,1)S(1)}, u32[]{:S(2)}, u32[]{:S(2)}) collective-permute-start(bf16[128,128]{0,1:T(8,128)(2,1)S(1)} %get-tuple-element.8), channel_id=1, source_target_pairs={{8,0},{16,8},{24,16},{32,24},{40,32},{48,40},{56,48},{64,56},{72,6... | collective-permute-start | bytes 98312 | tf_op jit(solution)/shard_map/ppermute | solution.py:22
  21.2 3.5 copy-start.2
  23.9 1.4 copy-start.7
  26.0 0.9 copy-start.3
  29.3 26.6 %all-to-all-start = ((bf16[8,768,128]{1,2,0:T(8,128)(2,1)}), bf16[8,768,128]{1,2,0:T(8,128)(2,1)S(1)}, u32[]{:S(2)}, u32[]{:S(2)}) async-start(bf16[8,768,128]{1,2,0:T(8,128)(2,1)} %broadcast_in_dim.73), calls=%async_computation | async-start | bytes 3145728 | tf_op jit(solution)/shard_map/all_to_all | solution.py:29
  35.3 177.7 %all-gather.4.cloned.1.call-start = ((), (), s32[]{:S(2)}) async-start(), calls=%async_computation.4 | async-start | bytes 14155776 | tf_op jit(solution)/shard_map/all_gather | solution.py:162
  63.2 0.8 copy-start.5
  64.9 1.7 copy-start.1
  145.1 79.6 %copy-start.9 = (bf16[1,2048,128]{2,1,0:T(8,128)(2,1)S(1)}, bf16[1,2048,128]{2,1,0:T(8,128)(2,1)}, u32[]{:S(2)}) copy-start(bf16[1,2048,128]{2,1,0:T(8,128)(2,1)} %param.26) | copy-start | bytes 1572868
  145.1 135.2 %all-gather.6.cloned.1.call-start = ((), (), s32[]{:S(2)}) async-start(), calls=%async_computation.5 | async-start | bytes 7077888 | tf_op jit(solution)/shard_map/all_gather | solution.py:173
  224.7 3.6 copy-start.10
  304.7 47.4 %all-to-all-start.2 = ((bf16[32,1,1,96,256]{4,3,2,1,0:T(8,128)(2,1)}), bf16[32,1,1,96,256]{4,3,2,1,0:T(8,128)(2,1)S(1)}, u32[]{:S(2)}, u32[]{:S(2)}) async-start(bf16[32,1,1,96,256]{4,3,2,1,0:T(8,128)(2,1)} %constant_dynamic-update-slice_fusion.2), calls=%async_computation.2 | async-start | bytes 3145728 | tf_op jit(solution)/shard_map/all_to_all | solution.py:178
  314.5 0.9 copy-start.6
  359.6 16.4 %copy-start.8 = (f32[256]{0:T(256)S(1)}, f32[256]{0:T(256)}, u32[]{:S(2)}) copy-start(f32[256]{0:T(256)} %param.29) | copy-start | bytes 3076
Sparse Core Ops, SparseCore 0:
  145.2 67.7 all-gather.3
  232.9 47.3 all-gather.5
